TPU v7x, 256 devices: a whole 4x4x8 slice. The times are simulated.
256 devices in a mesh: sp: 64 (over z, x, core), tp: 4 (over y).
Axes of the slice: x: 4, y: 4, z: 8, core: 2. Of those that a mesh axis runs over, the one named last changes fastest.
Arguments:
- tokens: bfloat16 [12288, 2048], P(('sp', 'tp')), may hold values from -54 to 54
- w_query: bfloat16 [2048, 2048], P(None, 'tp'), may hold values from -0.21875 to 0.21875
- w_key: bfloat16 [2048, 2048], P(None, 'tp'), may hold values from -0.125 to 0.125
- w_value: bfloat16 [2048, 2048], P(None, 'tp'), may hold values from -0.125 to 0.125
- w_out: bfloat16 [2048, 2048], P('tp'), may hold values from -0.125 to 0.125
- mix_weight: float32 [16], P('tp'), may hold values from 0.3 to 0.8
- out_gain: float32 [128], replicated, may hold values from 0.1 to 1.9
Outputs:
- mixed: bfloat16 [12288, 2048], P(('sp', 'tp'))
All inputs are finite; a program needn't handle non-finite values.
Results may differ from a plain program's by a relative error of at most 0.018.
The roundings to bfloat16 on the way count: a program that leaves them out, or rounds other values in their place, can miss the bound.
Values may be sent and summed in bfloat16 or wider, within the bound.
A program may use at most 192 MiB of HBM per device.

v0:
```python
import jax
import jax.numpy as jnp
from jax import lax
from jax.sharding import PartitionSpec as P


def in_order(tiles, dim):
    lengths = list(tiles.shape[1:])
    lengths[dim] *= tiles.shape[0]
    return jnp.moveaxis(tiles, 0, dim).reshape(lengths)


def from_everyone(shard, axis):
    copies = jnp.broadcast_to(shard, (lax.axis_size(axis), *shard.shape))
    return lax.all_to_all(copies, axis, split_axis=0, concat_axis=0, tiled=True)


def gathered_copies(shard, axis, dim):
    return in_order(from_everyone(shard, axis), dim)


def split_up(shard, dim, count):
    lengths = shard.shape
    tiles = shard.reshape(*lengths[:dim], count, lengths[dim] // count, *lengths[dim + 1 :])
    return jnp.moveaxis(tiles, dim, 0)


def sum_at_owner(shard, axis, dim):
    count = lax.axis_size(axis)
    tiles = lax.all_to_all(split_up(shard, dim, count), axis, 0, 0, tiled=True)
    return jnp.sum(tiles.astype(jnp.float32), axis=0)


def block_rows(rows):
    best = 1
    for candidate in range(1, rows + 1):
        if rows % candidate == 0 and candidate <= 2048:
            best = candidate
    return best


def shards(tokens, w_query, w_key, w_value, w_out, mix_weight, out_gain):
    query_cols = w_query.shape[1]
    key_cols = w_key.shape[1]
    heads_here = mix_weight.shape[0]
    head_dim = query_cols // (2 * heads_here)
    value_dim = w_value.shape[1] // heads_here
    piece = gathered_copies(tokens, "tp", 0)
    part_q = jnp.dot(piece, w_query, preferred_element_type=jnp.float32).astype(jnp.bfloat16)
    part_k = jnp.dot(piece, w_key, preferred_element_type=jnp.float32).astype(jnp.bfloat16)
    part_v = jnp.dot(piece, w_value, preferred_element_type=jnp.float32).astype(jnp.bfloat16)
    joined = jnp.concatenate([part_q, part_k, part_v], axis=1)
    queries = joined[:, :query_cols]
    keys = joined[:, query_cols : query_cols + key_cols]
    values = joined[:, query_cols + key_cols :]
    n_query = queries.shape[0]
    query_four = queries.reshape(n_query, heads_here, 2, head_dim)
    scale = head_dim ** (-0.5)

    def step(carry, block):
        running_max, running_sum, accum = carry
        key_blk, value_blk = block
        scores = (
            jnp.einsum("qhmd,khmd->hmqk", query_four, key_blk, preferred_element_type=jnp.float32)
            * scale
        )
        new_max = jnp.maximum(running_max, jnp.max(scores, axis=-1))
        factor = jnp.exp(running_max - new_max)
        expw = jnp.exp(scores - new_max[..., None])
        running_sum = running_sum * factor + jnp.sum(expw, axis=-1)
        weights = expw.astype(jnp.bfloat16)
        accum = accum * factor[..., None] + jnp.einsum(
            "hmqk,khe->hmqe", weights, value_blk, preferred_element_type=jnp.float32
        )
        return ((new_max, running_sum, accum), None)

    initial = (
        jnp.full((heads_here, 2, n_query), -1e30, jnp.float32),
        jnp.zeros((heads_here, 2, n_query), jnp.float32),
        jnp.zeros((heads_here, 2, n_query, value_dim), jnp.float32),
    )
    all_keys, all_values = (
        lax.all_gather(keys, "sp", axis=0, tiled=True),
        lax.all_gather(values, "sp", axis=0, tiled=True),
    )
    carry = initial
    rows = all_keys.shape[0]
    group = block_rows(rows)
    key_blocks = all_keys.reshape(rows // group, group, heads_here, 2, head_dim)
    value_blocks = all_values.reshape(rows // group, group, heads_here, value_dim)
    carry, unused = lax.scan(step, carry, (key_blocks, value_blocks))
    running_max, running_sum, accum = carry
    heads_out = (
        accum[:, 0] / running_sum[:, 0, :, None]
        - mix_weight[:, None, None] * accum[:, 1] / running_sum[:, 1, :, None]
    )
    meansq = jnp.mean(heads_out * heads_out, axis=-1, keepdims=True)
    normed = (heads_out * lax.rsqrt(meansq + 1e-06) * out_gain).astype(jnp.bfloat16)
    normed = normed.transpose(1, 0, 2).reshape(n_query, heads_here * value_dim)
    summed = sum_at_owner(
        jnp.dot(normed, w_out, preferred_element_type=jnp.float32).astype(jnp.bfloat16), "tp", 0
    )
    return summed.astype(jnp.bfloat16)


def solution(mesh):
    in_specs = (
        P(("sp", "tp"), None),
        P(None, "tp"),
        P(None, "tp"),
        P(None, "tp"),
        P("tp", None),
        P("tp"),
        P(),
    )
    out_specs = P(("sp", "tp"), None)
    return jax.shard_map(shards, mesh=mesh, in_specs=in_specs, out_specs=out_specs, check_vma=False)
```

profile of v0, /device:TPU:1, one launch (start us, length us, event | category | flops | bytes accessed | tf_op | source)
XLA Modules:
  0.0 394.2 jit_solution(17706083534486935025)
XLA Ops:
  6.5 0.0 copy-start
  6.5 0.0 all-gather.3.cloned.1.call-start
  6.5 1.1 broadcast_in_dim.20
  7.7 16.2 %all_to_all.10 = bf16[4,48,2048]{2,1,0:T(8,128)(2,1)S(1)} all-to-all(bf16[4,48,2048]{2,1,0:T(8,128)(2,1)S(1)} %broadcast_in_dim.20), channel_id=1, replica_groups=mesh['sp'=64,'tp'=4] {'tp'}, dimensions={0} | all-to-all | bytes 1572864 | tf_op jit(solution)/shard_map/all_to_all | solution.py:15
  23.9 2.8 convolution_convert_fusion.3
  26.8 0.0 all-gather.3.cloned.1.call-update
  26.8 0.0 all-gather.5.cloned.1.call-start
  26.9 2.9 convolution_convert_fusion.1
  29.7 0.0 all-gather.5.cloned.1.call-update
  29.8 2.2 convolution_convert_fusion.2
  31.9 0.1 copy.13
  32.1 86.8 %all-gather.3.cloned.1.call-done = bf16[12288,512]{1,0:T(8,128)(2,1)} async-done(((bf16[192,512]{1,0:T(8,128)(2,1)}), bf16[12288,512]{1,0:T(8,128)(2,1)}) %all-gather.3.cloned.1.call-update) | async-done | bytes 12582928 | tf_op jit(solution)/shard_map/all_gather | solution.py:83
  118.9 44.6 %reshape.39 = bf16[6,2048,4,2,64]{4,3,2,1,0:T(2,128)(2,1)} reshape(bf16[12288,512]{1,0:T(8,128)(2,1)} %all-gather.3.cloned.1.call-done) | data formatting | bytes 25165824 | tf_op jit(solution)/shard_map/reshape | solution.py:89
  163.5 58.6 %copy.14 = bf16[6,2048,4,2,64]{1,4,3,2,0:T(8,128)(2,1)} copy(bf16[6,2048,4,2,64]{4,3,2,1,0:T(2,128)(2,1)} %reshape.39) | data formatting | bytes 25165824
  222.2 0.0 all-gather.5.cloned.1.call-done
  222.2 18.1 %reshape.35 = bf16[6,2048,4,128]{3,2,1,0:T(4,128)(2,1)} reshape(bf16[12288,512]{1,0:T(8,128)(2,1)} %all-gather.5.cloned.1.call-done) | data formatting | bytes 25165824 | tf_op jit(solution)/shard_map/reshape | solution.py:90
  240.3 0.0 copy-start.2
  240.3 0.0 copy-start.3
  240.3 128.2 %while.15 = (s32[]{:T(128)}, f32[4,2,192]{2,1,0:T(2,128)S(1)}, f32[4,2,192]{2,1,0:T(2,128)S(1)}, f32[4,2,192,128]{3,2,1,0:T(8,128)}, bf16[6,2048,4,2,64]{1,4,3,2...) while((s32[]{:T(128)}, f32[4,2,192]{2,1,0:T(2,128)S(1)}, ...), condition=%wide.region_3.4_spmd.clone, body=%wide.region_0.3_spmd.clone.sunk | while | flops 1233722880 | bytes 98337416 | solution.py:91
  240.3 7.9 %bitcast_reduce_fusion.2 = (f32[4,2,192]{2,1,0:T(2,128)S(1)}, f32[4,2,2048,192]{2,3,1,0:T(8,128)}) fusion(bf16[192,4,2,64]{0,3,2,1:T(8,128)(2,1)S(1)} %get-tuple-element.181, bf16[6,2048,4,2,64]{1,4,3,2,0:T(8,128)(2,1)} %get-tuple-element.180, s32[]{:T(128)} %get-tuple-element.167), kind=kOutput, calls=%fused_computation.1.clone.1 | convolution fusion | flops 408943104 | bytes 14883328 | tf_op jit(solution)/shard_map/while/body/eval_jaxpr/qhmd,khmd->hmqk/dot_general | solution.py:64
  248.2 0.0 copy-start.1
  248.2 6.9 %fusion.45 = f32[4,2,192]{2,1,0:T(2,128)S(1)} fusion(f32[4,2,2048,192]{2,3,1,0:T(8,128)} %get-tuple-element.155, f32[4,2,192]{2,1,0:T(2,128)S(1)} %fusion.44), kind=kLoop, calls=%fused_computation.4.clone.1 | loop fusion | flops 9435648 | bytes 12595200 | tf_op jit(solution)/shard_map/while/body/eval_jaxpr/reduce_sum | solution.py:70
  255.2 2.2 constant_dynamic-slice_fusion.2
  257.4 0.0 copy-done.1
  257.4 3.5 fusion.47
  260.9 7.9 %bitcast_reduce_fusion.2 = (f32[4,2,192]{2,1,0:T(2,128)S(1)}, f32[4,2,2048,192]{2,3,1,0:T(8,128)}) fusion(bf16[192,4,2,64]{0,3,2,1:T(8,128)(2,1)S(1)} %get-tuple-element.181, bf16[6,2048,4,2,64]{1,4,3,2,0:T(8,128)(2,1)} %get-tuple-element.180, s32[]{:T(128)} %get-tuple-element.167), kind=kOutput, calls=%fused_computation.1.clone.1 | convolution fusion | flops 408943104 | bytes 14883328 | tf_op jit(solution)/shard_map/while/body/eval_jaxpr/qhmd,khmd->hmqk/dot_general | solution.py:64
  268.8 0.0 copy-start.1
  268.8 6.9 %fusion.45 = f32[4,2,192]{2,1,0:T(2,128)S(1)} fusion(f32[4,2,2048,192]{2,3,1,0:T(8,128)} %get-tuple-element.155, f32[4,2,192]{2,1,0:T(2,128)S(1)} %fusion.44), kind=kLoop, calls=%fused_computation.4.clone.1 | loop fusion | flops 9435648 | bytes 12595200 | tf_op jit(solution)/shard_map/while/body/eval_jaxpr/reduce_sum | solution.py:70
  275.8 2.2 constant_dynamic-slice_fusion.2
  277.9 0.0 copy-done.1
  277.9 4.5 %fusion.47 = f32[4,2,192,128]{3,2,1,0:T(8,128)} fusion(bf16[1,2048,4,128]{3,2,1,0:T(4,128)(2,1)S(1)} %constant_dynamic-slice_fusion.2, f32[4,2,2048,192]{2,3,1,0:T(8,128)S(1)} %copy-done.1, f32[4,2,192]{2,1,0:T(2,128)S(1)} %fusion.44, f32[4,2,192,128]{3,2,1,0:T(8,128)} %get-tuple-element.170, f32[4,2,192]{2,1,0:T(2,128)S(1)} %get-tuple-element.157, ...), kind=kOutput, calls=%fused_computation.12.clone.1 | convolution fusion | flops 815333376 | bytes 16265217 | tf_op jit(solution)/shard_map/while/body/eval_jaxpr/hmqk,khe->hmqe/dot_general | solution.py:72
  282.4 7.9 %bitcast_reduce_fusion.2 = (f32[4,2,192]{2,1,0:T(2,128)S(1)}, f32[4,2,2048,192]{2,3,1,0:T(8,128)}) fusion(bf16[192,4,2,64]{0,3,2,1:T(8,128)(2,1)S(1)} %get-tuple-element.181, bf16[6,2048,4,2,64]{1,4,3,2,0:T(8,128)(2,1)} %get-tuple-element.180, s32[]{:T(128)} %get-tuple-element.167), kind=kOutput, calls=%fused_computation.1.clone.1 | convolution fusion | flops 408943104 | bytes 14883328 | tf_op jit(solution)/shard_map/while/body/eval_jaxpr/qhmd,khmd->hmqk/dot_general | solution.py:64
  290.3 0.0 copy-start.1
  290.3 6.9 %fusion.45 = f32[4,2,192]{2,1,0:T(2,128)S(1)} fusion(f32[4,2,2048,192]{2,3,1,0:T(8,128)} %get-tuple-element.155, f32[4,2,192]{2,1,0:T(2,128)S(1)} %fusion.44), kind=kLoop, calls=%fused_computation.4.clone.1 | loop fusion | flops 9435648 | bytes 12595200 | tf_op jit(solution)/shard_map/while/body/eval_jaxpr/reduce_sum | solution.py:70
  297.3 2.2 constant_dynamic-slice_fusion.2
  299.5 0.0 copy-done.1
  299.5 4.5 %fusion.47 = f32[4,2,192,128]{3,2,1,0:T(8,128)} fusion(bf16[1,2048,4,128]{3,2,1,0:T(4,128)(2,1)S(1)} %constant_dynamic-slice_fusion.2, f32[4,2,2048,192]{2,3,1,0:T(8,128)S(1)} %copy-done.1, f32[4,2,192]{2,1,0:T(2,128)S(1)} %fusion.44, f32[4,2,192,128]{3,2,1,0:T(8,128)} %get-tuple-element.170, f32[4,2,192]{2,1,0:T(2,128)S(1)} %get-tuple-element.157, ...), kind=kOutput, calls=%fused_computation.12.clone.1 | convolution fusion | flops 815333376 | bytes 16265217 | tf_op jit(solution)/shard_map/while/body/eval_jaxpr/hmqk,khe->hmqe/dot_general | solution.py:72
  303.9 7.9 %bitcast_reduce_fusion.2 = (f32[4,2,192]{2,1,0:T(2,128)S(1)}, f32[4,2,2048,192]{2,3,1,0:T(8,128)}) fusion(bf16[192,4,2,64]{0,3,2,1:T(8,128)(2,1)S(1)} %get-tuple-element.181, bf16[6,2048,4,2,64]{1,4,3,2,0:T(8,128)(2,1)} %get-tuple-element.180, s32[]{:T(128)} %get-tuple-element.167), kind=kOutput, calls=%fused_computation.1.clone.1 | convolution fusion | flops 408943104 | bytes 14883328 | tf_op jit(solution)/shard_map/while/body/eval_jaxpr/qhmd,khmd->hmqk/dot_general | solution.py:64
  311.9 0.0 copy-start.1
  311.9 6.9 %fusion.45 = f32[4,2,192]{2,1,0:T(2,128)S(1)} fusion(f32[4,2,2048,192]{2,3,1,0:T(8,128)} %get-tuple-element.155, f32[4,2,192]{2,1,0:T(2,128)S(1)} %fusion.44), kind=kLoop, calls=%fused_computation.4.clone.1 | loop fusion | flops 9435648 | bytes 12595200 | tf_op jit(solution)/shard_map/while/body/eval_jaxpr/reduce_sum | solution.py:70
  318.8 2.2 constant_dynamic-slice_fusion.2
  321.0 0.0 copy-done.1
  321.0 4.5 %fusion.47 = f32[4,2,192,128]{3,2,1,0:T(8,128)} fusion(bf16[1,2048,4,128]{3,2,1,0:T(4,128)(2,1)S(1)} %constant_dynamic-slice_fusion.2, f32[4,2,2048,192]{2,3,1,0:T(8,128)S(1)} %copy-done.1, f32[4,2,192]{2,1,0:T(2,128)S(1)} %fusion.44, f32[4,2,192,128]{3,2,1,0:T(8,128)} %get-tuple-element.170, f32[4,2,192]{2,1,0:T(2,128)S(1)} %get-tuple-element.157, ...), kind=kOutput, calls=%fused_computation.12.clone.1 | convolution fusion | flops 815333376 | bytes 16265217 | tf_op jit(solution)/shard_map/while/body/eval_jaxpr/hmqk,khe->hmqe/dot_general | solution.py:72
  325.5 7.9 %bitcast_reduce_fusion.2 = (f32[4,2,192]{2,1,0:T(2,128)S(1)}, f32[4,2,2048,192]{2,3,1,0:T(8,128)}) fusion(bf16[192,4,2,64]{0,3,2,1:T(8,128)(2,1)S(1)} %get-tuple-element.181, bf16[6,2048,4,2,64]{1,4,3,2,0:T(8,128)(2,1)} %get-tuple-element.180, s32[]{:T(128)} %get-tuple-element.167), kind=kOutput, calls=%fused_computation.1.clone.1 | convolution fusion | flops 408943104 | bytes 14883328 | tf_op jit(solution)/shard_map/while/body/eval_jaxpr/qhmd,khmd->hmqk/dot_general | solution.py:64
  333.4 0.0 copy-start.1
  333.4 6.9 %fusion.45 = f32[4,2,192]{2,1,0:T(2,128)S(1)} fusion(f32[4,2,2048,192]{2,3,1,0:T(8,128)} %get-tuple-element.155, f32[4,2,192]{2,1,0:T(2,128)S(1)} %fusion.44), kind=kLoop, calls=%fused_computation.4.clone.1 | loop fusion | flops 9435648 | bytes 12595200 | tf_op jit(solution)/shard_map/while/body/eval_jaxpr/reduce_sum | solution.py:70
  340.4 2.2 constant_dynamic-slice_fusion.2
  342.5 0.0 copy-done.1
  342.5 4.5 %fusion.47 = f32[4,2,192,128]{3,2,1,0:T(8,128)} fusion(bf16[1,2048,4,128]{3,2,1,0:T(4,128)(2,1)S(1)} %constant_dynamic-slice_fusion.2, f32[4,2,2048,192]{2,3,1,0:T(8,128)S(1)} %copy-done.1, f32[4,2,192]{2,1,0:T(2,128)S(1)} %fusion.44, f32[4,2,192,128]{3,2,1,0:T(8,128)} %get-tuple-element.170, f32[4,2,192]{2,1,0:T(2,128)S(1)} %get-tuple-element.157, ...), kind=kOutput, calls=%fused_computation.12.clone.1 | convolution fusion | flops 815333376 | bytes 16265217 | tf_op jit(solution)/shard_map/while/body/eval_jaxpr/hmqk,khe->hmqe/dot_general | solution.py:72
  347.0 7.9 %bitcast_reduce_fusion.2 = (f32[4,2,192]{2,1,0:T(2,128)S(1)}, f32[4,2,2048,192]{2,3,1,0:T(8,128)}) fusion(bf16[192,4,2,64]{0,3,2,1:T(8,128)(2,1)S(1)} %get-tuple-element.181, bf16[6,2048,4,2,64]{1,4,3,2,0:T(8,128)(2,1)} %get-tuple-element.180, s32[]{:T(128)} %get-tuple-element.167), kind=kOutput, calls=%fused_computation.1.clone.1 | convolution fusion | flops 408943104 | bytes 14883328 | tf_op jit(solution)/shard_map/while/body/eval_jaxpr/qhmd,khmd->hmqk/dot_general | solution.py:64
  354.9 0.0 copy-start.1
  354.9 6.9 %fusion.45 = f32[4,2,192]{2,1,0:T(2,128)S(1)} fusion(f32[4,2,2048,192]{2,3,1,0:T(8,128)} %get-tuple-element.155, f32[4,2,192]{2,1,0:T(2,128)S(1)} %fusion.44), kind=kLoop, calls=%fused_computation.4.clone.1 | loop fusion | flops 9435648 | bytes 12595200 | tf_op jit(solution)/shard_map/while/body/eval_jaxpr/reduce_sum | solution.py:70
  361.9 2.2 constant_dynamic-slice_fusion.2
  364.1 0.0 copy-done.1
  364.1 4.5 %fusion.47 = f32[4,2,192,128]{3,2,1,0:T(8,128)} fusion(bf16[1,2048,4,128]{3,2,1,0:T(4,128)(2,1)S(1)} %constant_dynamic-slice_fusion.2, f32[4,2,2048,192]{2,3,1,0:T(8,128)S(1)} %copy-done.1, f32[4,2,192]{2,1,0:T(2,128)S(1)} %fusion.44, f32[4,2,192,128]{3,2,1,0:T(8,128)} %get-tuple-element.170, f32[4,2,192]{2,1,0:T(2,128)S(1)} %get-tuple-element.157, ...), kind=kOutput, calls=%fused_computation.12.clone.1 | convolution fusion | flops 815333376 | bytes 16265217 | tf_op jit(solution)/shard_map/while/body/eval_jaxpr/hmqk,khe->hmqe/dot_general | solution.py:72
  368.6 0.0 copy-done.2
  368.6 1.6 multiply_reduce_fusion
  370.2 0.0 copy-done
  370.2 0.0 copy-done.3
  370.2 0.6 convolution_convert_fusion
  370.9 15.6 %all_to_all.11 = bf16[4,48,2048]{2,1,0:T(8,128)(2,1)S(1)} all-to-all(bf16[4,48,2048]{2,1,0:T(8,128)(2,1)S(1)} %bitcast.78), channel_id=1, replica_groups=mesh['sp'=64,'tp'=4] {'tp'}, dimensions={0} | all-to-all | bytes 1572864 | tf_op jit(solution)/shard_map/all_to_all | solution.py:30
  386.5 0.8 reduce_sum.31
  (24 shorter events, 0.3 us)
Async XLA Ops:
  6.5 363.7 %copy-start = (bf16[512,2048]{1,0:T(8,128)(2,1)S(1)}, bf16[512,2048]{1,0:T(8,128)(2,1)}, u32[]{:S(2)}) copy-start(bf16[512,2048]{1,0:T(8,128)(2,1)} %param.13) | copy-start | bytes 6291460
  6.5 112.4 %all-gather.3.cloned.1.call-start = ((), (), s32[]{:S(2)}) async-start(), calls=%async_computation.2 | async-start | bytes 12779520 | tf_op jit(solution)/shard_map/all_gather | solution.py:83
  26.8 195.4 %all-gather.5.cloned.1.call-start = ((), (), s32[]{:S(2)}) async-start(), calls=%async_computation.3 | async-start | bytes 12779520 | tf_op jit(solution)/shard_map/all_gather | solution.py:84
  240.3 128.3 %copy-start.2 = (f32[4]{0:T(128)S(1)}, f32[4]{0:T(128)}, u32[]{:S(2)}) copy-start(f32[4]{0:T(128)} %param.14) | copy-start | bytes 52
  240.3 129.9 %copy-start.3 = (f32[128]{0:T(128)S(1)}, f32[128]{0:T(128)}, u32[]{:S(2)}) copy-start(f32[128]{0:T(128)} %param.15) | copy-start | bytes 1540
  248.2 9.1 %copy-start.1 = (f32[4,2,2048,192]{2,3,1,0:T(8,128)S(1)}, f32[4,2,2048,192]{2,3,1,0:T(8,128)}, u32[]{:S(2)}) copy-start(f32[4,2,2048,192]{2,3,1,0:T(8,128)} %get-tuple-element.155) | copy-start | bytes 37748740 | tf_op jit(solution)/shard_map/while
  268.8 9.1 %copy-start.1 = (f32[4,2,2048,192]{2,3,1,0:T(8,128)S(1)}, f32[4,2,2048,192]{2,3,1,0:T(8,128)}, u32[]{:S(2)}) copy-start(f32[4,2,2048,192]{2,3,1,0:T(8,128)} %get-tuple-element.155) | copy-start | bytes 37748740 | tf_op jit(solution)/shard_map/while
  290.3 9.1 %copy-start.1 = (f32[4,2,2048,192]{2,3,1,0:T(8,128)S(1)}, f32[4,2,2048,192]{2,3,1,0:T(8,128)}, u32[]{:S(2)}) copy-start(f32[4,2,2048,192]{2,3,1,0:T(8,128)} %get-tuple-element.155) | copy-start | bytes 37748740 | tf_op jit(solution)/shard_map/while
  311.9 9.1 %copy-start.1 = (f32[4,2,2048,192]{2,3,1,0:T(8,128)S(1)}, f32[4,2,2048,192]{2,3,1,0:T(8,128)}, u32[]{:S(2)}) copy-start(f32[4,2,2048,192]{2,3,1,0:T(8,128)} %get-tuple-element.155) | copy-start | bytes 37748740 | tf_op jit(solution)/shard_map/while
  333.4 9.1 %copy-start.1 = (f32[4,2,2048,192]{2,3,1,0:T(8,128)S(1)}, f32[4,2,2048,192]{2,3,1,0:T(8,128)}, u32[]{:S(2)}) copy-start(f32[4,2,2048,192]{2,3,1,0:T(8,128)} %get-tuple-element.155) | copy-start | bytes 37748740 | tf_op jit(solution)/shard_map/while
  354.9 9.1 %copy-start.1 = (f32[4,2,2048,192]{2,3,1,0:T(8,128)S(1)}, f32[4,2,2048,192]{2,3,1,0:T(8,128)}, u32[]{:S(2)}) copy-start(f32[4,2,2048,192]{2,3,1,0:T(8,128)} %get-tuple-element.155) | copy-start | bytes 37748740 | tf_op jit(solution)/shard_map/while
Sparse Core Ops, SparseCore 0:
  26.9 91.9 all-gather.2
  121.7 86.3 all-gather.4
where the time goes:
time: 398 us; the launch traced here: 394 us
  local copies, waits for them, and re-layouts  136 us (34%)
  waiting for transfers between devices  86.8 us (22%)
  matrix products  81.7 us (21%)
  other arithmetic  44.3 us (11%)
  blocking collectives  31.9 us (8%)
  between operations  13.5 us (3%)
    all_gather x1, waiting for transfers between devices, shards(): lax.all_gather(keys, 'sp', axis=0, tiled=True)  86.8 us
    unnamed x8, local copies, waits for them, and re-layouts  58.7 us
    dot_general x6, matrix products, step(): jnp.einsum('qhmd,khmd->hmqk', query_four, key_blk, preferred_element_type...  47.4 us
    reshape x1, local copies, waits for them, and re-layouts, shards(): key_blocks = all_keys.reshape(rows // group, group, heads_here, 2, head_dim)  44.6 us
    reduce_sum x6, other arithmetic, step(): running_sum = running_sum * factor + jnp.sum(expw, axis=-1)  41.6 us
    dot_general x6, matrix products, step(): jnp.einsum('hmqk,khe->hmqe', weights, value_blk, preferred_element_type=j...  25.8 us
    reshape x1, local copies, waits for them, and re-layouts, shards(): all_values.reshape(rows // group, group, heads_here, value_dim)  18.1 us
    all_to_all x1, blocking collectives, from_everyone(): return lax.all_to_all(copies, axis, split_axis=0, concat_axis=0, tiled=True)  16.2 us
  transfers between devices with their start and end apart: 2, of which 1 were waited for; matrix products, arithmetic and copies ran while one was open for 28% of the time, Pallas kernels for 0%

commit v1 on v0

v1 whole, which is shorter than its diff:
```python
import functools

import jax
import jax.numpy as jnp
from jax import lax
from jax.experimental import pallas as pl
from jax.experimental.pallas import tpu as pltpu
from jax.sharding import PartitionSpec as P

MESH = pl.DeviceIdType.MESH
NX = 4
NY = 4
NC = 2
Y_OFFSET = (0, 1, 3, 2)
BF16 = jnp.bfloat16
F32 = jnp.float32


def kernel(
    nz,
    rows,
    tok_hbm,
    wq_hbm,
    wk_hbm,
    wv_hbm,
    wo_hbm,
    lam_ref,
    gain_ref,
    out_ref,
    tok,
    wkvq,
    wo,
    send_kv,
    send_q,
    qbuf,
    kv,
    qw,
    top,
    total,
    acc,
    nbuf,
    mixin,
    load_sem,
    y_send,
    y_recv,
    x_send,
    x_recv,
    q_send,
    q_recv,
    r_send,
    r_recv,
    s_send,
    s_recv,
    wo_send,
    wo_recv,
    ws_send,
    ws_recv,
    o_send,
    o_recv,
):
    half = nz // 2
    whole_events = (half - 1) * 4
    events = whole_events + 2
    depth = tok.shape[-1]
    group = NX * rows
    queries = NY * group
    tiles = queries // 128
    out_rows = wo_hbm.shape[0]
    out_cols = wo.shape[-1]

    sp = lax.axis_index("sp")
    y = lax.axis_index("tp")
    c = lax.rem(sp, NC)
    x = lax.rem(sp // NC, NX)
    z = sp // (NC * NX)

    def device(zz, xx, cc, yy):
        return {"sp": (zz * NX + xx) * NC + cc, "tp": yy}

    def around(value, step, count):
        return lax.rem(value + (step % count), count)

    def remote(src, dst, send, recv, where):
        return pltpu.make_async_remote_copy(
            src_ref=src,
            dst_ref=dst,
            send_sem=send,
            recv_sem=recv,
            device_id=where,
            device_id_type=MESH,
        )

    up = device(z, x, c, around(y, 1, NY))
    down = device(z, x, c, around(y, -1, NY))
    right = device(around(z, 1, nz), x, c, y)
    left = device(around(z, -1, nz), x, c, y)
    sibling = device(z, x, 1 - c, y)

    loads = []
    for part in range(2):
        loads.append(
            pltpu.make_async_copy(
                tok_hbm.at[:, pl.ds(part * depth, depth)], tok.at[0, part], load_sem.at[part]
            )
        )
    weight_loads = [
        pltpu.make_async_copy(w, wkvq.at[i], load_sem.at[2 + i])
        for i, w in enumerate((wk_hbm, wv_hbm, wq_hbm))
    ]
    wo_loads = [
        pltpu.make_async_copy(
            wo_hbm.at[:, pl.ds(part * out_cols, out_cols)], wo.at[y, part], load_sem.at[5 + part]
        )
        for part in range(2)
    ]
    for copy in loads + weight_loads + wo_loads:
        copy.start()

    barrier = pltpu.get_barrier_semaphore()
    peers = [right, left, sibling]
    for oy in range(NY):
        for ox in range(NX):
            if (oy, ox) != (0, 0):
                peers.append(device(z, around(x, ox, NX), c, around(y, oy, NY)))
    for peer in peers:
        pl.semaphore_signal(barrier, inc=1, device_id=peer, device_id_type=MESH)
    for copy in loads:
        copy.wait()
    pl.semaphore_wait(barrier, len(peers))

    def y_copy(slot, part):
        return remote(
            tok.at[0, part],
            tok.at[slot, part],
            y_send.at[slot, part],
            y_recv.at[slot, part],
            down if slot == 1 else up,
        )

    def y_relay(part):
        return remote(
            tok.at[2 if part == 0 else 1, part],
            tok.at[3, part],
            y_send.at[3, part],
            y_recv.at[3, part],
            up if part == 0 else down,
        )

    y_copy(2, 0).start()
    y_copy(1, 1).start()
    y_copy(2, 1).start()
    y_copy(1, 0).start()

    def x_copies(s, o):
        other = around(x, o, NX)
        source = around(x, -o, NX)
        to = device(z, other, c, y)
        mine = pl.ds(pl.multiple_of(s * group + x * rows, 16), rows)
        theirs = pl.ds(pl.multiple_of(s * group + source * rows, 16), rows)
        return (
            remote(send_kv.at[s, other], kv.at[0, mine], x_send.at[s, o], x_recv.at[s, o], to),
            remote(send_q.at[s, other], qbuf.at[mine], q_send.at[s, o], q_recv.at[s, o], to),
            remote(send_kv.at[s, other], kv.at[0, theirs], x_send.at[s, o], x_recv.at[s, o], to),
            remote(send_q.at[s, other], qbuf.at[theirs], q_send.at[s, o], q_recv.at[s, o], to),
        )

    def project(s):
        first = tok[s, 0]
        second = tok[s, 1]

        def product(i):
            out = jnp.dot(first, wkvq[i, :depth, :], preferred_element_type=F32)
            out += jnp.dot(second, wkvq[i, depth:, :], preferred_element_type=F32)
            return out.astype(BF16)

        mine = pl.ds(pl.multiple_of(s * group + x * rows, 16), rows)
        keys = product(0)
        values = product(1)
        for head in range(NX):
            cols = slice(head * 128, head * 128 + 128)
            send_kv[s, head, :, :128] = keys[:, cols]
            send_kv[s, head, :, 128:] = values[:, cols]
        for o in (2, 1, 3):
            x_copies(s, o)[0].start()
        kv[0, mine, :] = send_kv[s, x]
        found = product(2)
        for head in range(NX):
            send_q[s, head] = found[:, head * 128 : head * 128 + 128]
        for o in (2, 1, 3):
            x_copies(s, o)[1].start()
        qbuf[mine, :] = send_q[s, x]

    def ring_first(s, way):
        if half > 1:
            event = s
        elif (way == 0) == (s < 2):
            event = s % 2
        else:
            return None
        return remote(
            kv.at[0, pl.ds(s * group, group)],
            kv.at[2 + event, pl.ds(way * group, group)],
            r_send.at[s, way],
            r_recv.at[event, way],
            right if way == 0 else left,
        )

    def sibling_first(s):
        span = pl.ds(s * group, group)
        return remote(kv.at[0, span], kv.at[1, span], s_send.at[events + s], s_recv.at[events + s], sibling)

    def launch(s):
        for o in (1, 3, 2):
            x_copies(s, o)[2].wait_recv()
        for way in range(2):
            copy = ring_first(s, way)
            if copy is not None:
                copy.start()
        sibling_first(s).start()

    for copy in weight_loads:
        copy.wait()
    project(0)
    launch(0)
    y_copy(2, 0).wait_recv()
    y_relay(0).start()
    y_copy(1, 1).wait_recv()
    y_relay(1).start()
    y_copy(1, 0).wait_recv()
    project(1)
    y_copy(2, 1).wait_recv()
    project(2)
    launch(1)
    launch(2)

    def wo_span(part):
        size = out_rows // 2
        return pl.ds(part * size, size)

    def wo_copy(way, part):
        span = wo_span(part)
        return remote(
            wo.at[y, c, span],
            wo.at[y, c, span],
            wo_send.at[way, part],
            wo_recv.at[way, part],
            up if way == 0 else down,
        )

    def wo_arrival(way, part):
        origin = around(y, -1 if way == 0 else 1, NY)
        span = wo_span(part)
        return remote(
            wo.at[y, c, span],
            wo.at[origin, c, span],
            wo_send.at[way, part],
            wo_recv.at[way, part],
            up if way == 0 else down,
        )

    def wo_relay(part):
        origin = around(y, -1 if part == 0 else 1, NY)
        span = wo_span(part)
        return remote(
            wo.at[origin, c, span],
            wo.at[origin, c, span],
            wo_send.at[2, part],
            wo_recv.at[2, part],
            up if part == 0 else down,
        )

    def wo_relay_arrival(part):
        origin = around(y, 2, NY)
        span = wo_span(part)
        return remote(
            wo.at[y, c, span],
            wo.at[origin, c, span],
            wo_send.at[2, part],
            wo_recv.at[2, part],
            up if part == 0 else down,
        )

    def wo_sibling(way, part, core):
        origin = around(y, (-1, 1, 2)[way], NY)
        span = wo_span(part)
        return remote(
            wo.at[origin, core, span],
            wo.at[origin, core, span],
            ws_send.at[way, part],
            ws_recv.at[way, part],
            sibling,
        )

    for copy in wo_loads:
        copy.wait()

    y_relay_in = [
        remote(tok.at[0, part], tok.at[3, part], y_send.at[3, part], y_recv.at[3, part], up)
        for part in range(2)
    ]
    for copy in y_relay_in:
        copy.wait_recv()
    wo_copy(0, 0).start()
    wo_copy(1, 1).start()
    wo_copy(0, 1).start()
    wo_copy(1, 0).start()
    project(3)
    launch(3)

    for s in range(NY):
        for o in (1, 3, 2):
            x_copies(s, o)[3].wait_recv()
    upper = lax.broadcasted_iota(jnp.int32, (128, 128), 0) < 64

    def build(t, carry):
        block = qbuf[pl.ds(pl.multiple_of(t * 128, 128), 128), :].astype(F32) * (64**-0.5)
        block = block.T
        nothing = jnp.zeros_like(block)
        qw[t, :, :128] = jnp.where(upper, block, nothing).astype(BF16)
        qw[t, :, 128:] = jnp.where(upper, nothing, block).astype(BF16)
        return carry

    lax.fori_loop(0, tiles, build, 0)
    top[...] = jnp.full_like(top, -1e30)
    total[...] = jnp.zeros_like(total)
    acc[...] = jnp.zeros_like(acc)

    def arrival(e, way):
        return remote(
            kv.at[0, pl.ds(0, group)],
            kv.at[2 + e, pl.ds(way * group, group)],
            r_send.at[e, way],
            r_recv.at[e, way],
            right,
        )

    def forward(e, way, target):
        return remote(
            kv.at[2 + e, pl.ds(way * group, group)],
            kv.at[2 + target, pl.ds(way * group, group)],
            r_send.at[4 + e, way],
            r_recv.at[target, way],
            right if way == 0 else left,
        )

    def to_sibling(e):
        return remote(
            kv.at[2 + e, pl.ds(0, 2 * group)],
            kv.at[2 + e, pl.ds(2 * group, 2 * group)],
            s_send.at[e],
            s_recv.at[e],
            sibling,
        )

    def goes_left(e):
        target = jnp.where(e + 4 < whole_events, e + 4, e + 2)
        return (e + 4 < whole_events) | ((e < whole_events) & (lax.rem(e, 4) >= 2)), target

    def receive(e):
        arrival(e, 0).wait_recv()

        @pl.when(e + 4 < events)
        def _():
            forward(e, 0, e + 4).start()

        arrival(e, 1).wait_recv()
        moves, target = goes_left(e)

        @pl.when(moves)
        def _():
            forward(e, 1, target).start()

        to_sibling(e).start()

    def attend(u, carry):
        @pl.when(u == 1)
        def _():
            for s in range(NY):
                sibling_first(s).wait_recv()

        @pl.when(u >= 2)
        def _():
            to_sibling(u - 2).wait_recv()

        keys = kv[u, :, :128]
        values = kv[u, :, 128:].T
        for t in range(tiles):
            scores = jnp.dot(keys, qw[t], preferred_element_type=F32)
            before = top[t]
            now = jnp.maximum(before, jnp.max(scores, axis=0, keepdims=True))
            factor = jnp.exp(before - now)
            expw = jnp.exp(scores - now)
            top[t] = now
            total[t] = total[t] * factor + jnp.sum(expw, axis=0, keepdims=True)
            acc[t] = acc[t] * factor + jnp.dot(values, expw.astype(BF16), preferred_element_type=F32)
        return carry

    relay_at = events // 2

    def step(e, carry):
        receive(e)

        @pl.when(e == relay_at)
        def _():
            for part in range(2):
                wo_arrival(part, part).wait_recv()
                wo_relay(part).start()
                wo_sibling(part, part, c).start()

        begin = e + jnp.where(e >= 5, 1, 0)
        end = e + 1 + jnp.where(e >= 4, 1, 0)
        lax.fori_loop(begin, end, attend, 0)
        return carry

    lax.fori_loop(0, events, step, 0)
    for way in range(2):
        wo_arrival(way, 1 - way).wait_recv()
        wo_sibling(way, 1 - way, c).start()
    behind = events + (1 if events > 4 else 0)
    lax.fori_loop(behind, events + 2, attend, 0)

    mix = lam_ref[x]
    gain = gain_ref[...]

    def finish(t, carry):
        ratio = acc[t] / total[t]
        heads_out = ratio[:, :128] - mix * ratio[:, 128:]
        meansq = jnp.mean(heads_out * heads_out, axis=0, keepdims=True)
        normed = (heads_out * lax.rsqrt(meansq + 1e-06)).T * gain
        nbuf[pl.ds(pl.multiple_of(t * 128, 128), 128), :] = normed.astype(BF16)
        return carry

    lax.fori_loop(0, tiles, finish, 0, unroll=True)

    def o_copy(s, o, arriving):
        other = around(x, o, NX)
        span = pl.ds(pl.multiple_of(s * group + other * rows, 16), rows)
        if arriving:
            slot = around(y, -Y_OFFSET[s], NY) * NX + around(x, -o, NX)
        else:
            slot = y * NX + x
        return remote(
            nbuf.at[span],
            mixin.at[slot],
            o_send.at[s, o],
            o_recv.at[s, o],
            device(z, other, c, around(y, Y_OFFSET[s], NY)),
        )

    exchanges = [(s, o) for s in (3, 1, 2, 0) for o in (2, 1, 3, 0) if (s, o) != (0, 0)]
    for s, o in exchanges:
        o_copy(s, o, False).start()
    mixin[y * NX + x] = nbuf[pl.ds(pl.multiple_of(x * rows, 16), rows), :]

    for part in range(2):
        wo_relay_arrival(part).wait_recv()
        wo_sibling(2, part, c).start()
    for way in range(3):
        for part in range(2):
            wo_sibling(way, part, 1 - c).wait_recv()
    for s, o in exchanges:
        o_copy(s, o, True).wait_recv()
    normed = jnp.concatenate([mixin[h] for h in range(NX * NY)], axis=1)
    for part in range(2):
        mixed = jnp.zeros((rows, out_cols), F32)
        for yy in range(NY):
            span = slice(yy * out_rows, (yy + 1) * out_rows)
            mixed += jnp.dot(normed[:, span], wo[yy, part], preferred_element_type=F32)
        out_ref[:, part * out_cols : (part + 1) * out_cols] = mixed.astype(BF16)

    for part in range(2):
        for slot in (1, 2):
            y_copy(slot, part).wait_send()
        y_relay(part).wait_send()
    for s in range(NY):
        for o in (1, 2, 3):
            copies = x_copies(s, o)
            copies[0].wait_send()
            copies[1].wait_send()
        for way in range(2):
            copy = ring_first(s, way)
            if copy is not None:
                copy.wait_send()
        sibling_first(s).wait_send()

    def drain(e, carry):
        @pl.when(e + 4 < events)
        def _():
            forward(e, 0, e + 4).wait_send()

        moves, target = goes_left(e)

        @pl.when(moves)
        def _():
            forward(e, 1, target).wait_send()

        to_sibling(e).wait_send()
        return carry

    lax.fori_loop(0, events, drain, 0)
    for part in range(2):
        for way in range(2):
            wo_copy(way, part).wait_send()
        wo_relay(part).wait_send()
        for way in range(3):
            wo_sibling(way, part, c).wait_send()
    for s, o in exchanges:
        o_copy(s, o, False).wait_send()


def solution(mesh):
    nz = mesh.shape["sp"] // (NX * NC)

    def shards(tokens, w_query, w_key, w_value, w_out, mix_weight, out_gain):
        rows, width = tokens.shape
        cols = w_query.shape[1]
        group = NX * rows
        queries = NY * group
        tiles = queries // 128
        events = (nz // 2 - 1) * 4 + 2
        dma = pltpu.SemaphoreType.DMA
        anywhere = pl.BlockSpec(memory_space=pl.ANY)
        return pl.pallas_call(
            functools.partial(kernel, nz, rows),
            out_shape=jax.ShapeDtypeStruct((rows, width), BF16),
            in_specs=[anywhere] * 5
            + [pl.BlockSpec(memory_space=pltpu.SMEM), pl.BlockSpec(memory_space=pltpu.VMEM)],
            out_specs=pl.BlockSpec(memory_space=pltpu.VMEM),
            scratch_shapes=[
                pltpu.VMEM((NY, 2, rows, width // 2), BF16),
                pltpu.VMEM((3, width, cols), BF16),
                pltpu.VMEM((NY, 2, w_out.shape[0], width // 2), BF16),
                pltpu.VMEM((NY, NX, rows, 256), BF16),
                pltpu.VMEM((NY, NX, rows, 128), BF16),
                pltpu.VMEM((queries, 128), BF16),
                pltpu.VMEM((events + 2, 4 * group, 256), BF16),
                pltpu.VMEM((tiles, 128, 256), BF16),
                pltpu.VMEM((tiles, 1, 256), F32),
                pltpu.VMEM((tiles, 1, 256), F32),
                pltpu.VMEM((tiles, 128, 256), F32),
                pltpu.VMEM((queries, 128), BF16),
                pltpu.VMEM((NX * NY, rows, 128), BF16),
                dma((7,)),
                dma((4, 2)),
                dma((4, 2)),
                dma((4, 4)),
                dma((4, 4)),
                dma((4, 4)),
                dma((4, 4)),
                dma((events + 4, 2)),
                dma((events, 2)),
                dma((events + 4,)),
                dma((events + 4,)),
                dma((3, 2)),
                dma((3, 2)),
                dma((3, 2)),
                dma((3, 2)),
                dma((4, 4)),
                dma((4, 4)),
            ],
            compiler_params=pltpu.CompilerParams(
                collective_id=0,
                has_side_effects=True,
                vmem_limit_bytes=56 * 1024 * 1024,
            ),
        )(tokens, w_query, w_key, w_value, w_out, mix_weight, out_gain.reshape(1, -1))

    in_specs = (
        P(("sp", "tp"), None),
        P(None, "tp"),
        P(None, "tp"),
        P(None, "tp"),
        P("tp", None),
        P("tp"),
        P(),
    )
    return jax.shard_map(
        shards, mesh=mesh, in_specs=in_specs, out_specs=P(("sp", "tp"), None), check_vma=False
    )
```

time: 398 us -> 91.7 us (0.23)
  local copies, waits for them, and re-layouts: 136 us -> 1.62 us
  Pallas kernels: 0 us -> 89.1 us
  waiting for transfers between devices: 86.8 us -> 0 us
  matrix products: 81.7 us -> 0 us
  other arithmetic: 44.3 us -> 0 us
  blocking collectives: 31.9 us -> 0 us
  between operations: 13.5 us -> 0.01 us
    pallas_call x0 -> x1, Pallas kernels: none -> 89.1 us  [shards(): pl.pallas_call(functools.partial(kernel, nz, rows), out_shape=jax.ShapeDt...]
    all_gather x2 -> x0, waiting for transfers between devices: 86.8 us -> none  [the longest x1 86.8 us: shards(): lax.all_gather(keys, 'sp', axis=0, tiled=True)]
    dot_general x16 -> x0, matrix products: 81.7 us -> none  [the longest x6 47.4 us: step(): jnp.einsum('qhmd,khmd->hmqk', query_four, key_blk, preferred_element_type...]
    reshape x2 -> x0, local copies, waits for them, and re-layouts: 62.8 us -> none  [the longest x1 44.6 us: shards(): key_blocks = all_keys.reshape(rows // group, group, heads_here, 2, head_dim)]
    unnamed x8 -> x1, local copies, waits for them, and re-layouts: 58.7 us -> 1.62 us
    reduce_sum x8 -> x0, other arithmetic: 44 us -> none  [the longest x6 41.6 us: step(): running_sum = running_sum * factor + jnp.sum(expw, axis=-1)]
    all_to_all x2 -> x0, blocking collectives: 31.9 us -> none  [the longest x1 16.2 us: from_everyone(): return lax.all_to_all(copies, axis, split_axis=0, concat_axis=0, tiled=True)]
    dynamic_slice x6 -> x0, local copies, waits for them, and re-layouts: 12.9 us -> none  [shards(): carry, unused = lax.scan(step, carry, (key_blocks, value_blocks))]
  transfers between devices with their start and end apart: 2 -> 0, of which waited for: 1 -> 0; matrix products, arithmetic and copies ran while one was open for 28% -> 0% of each run, Pallas kernels for 0% -> 0%
where the time goes in v1:
time: 91.7 us; the launch traced here: 90.7 us
  Pallas kernels  89.1 us (97%)
  local copies, waits for them, and re-layouts  1.62 us (2%)
    pallas_call x1, Pallas kernels, shards(): pl.pallas_call(functools.partial(kernel, nz, rows), out_shape=jax.ShapeDt...  89.1 us

profile of v1, /device:TPU:1, one launch (start us, length us, event | category | flops | bytes accessed | tf_op | source)
XLA Modules:
  0.0 90.7 jit_solution(8739409641475439176)
XLA Ops:
  0.0 89.1 %shard_map.73 = bf16[48,2048]{1,0:T(8,128)(2,1)} custom-call(bf16[48,2048]{1,0:T(8,128)(2,1)} %tok_hbm.1, bf16[2048,512]{1,0:T(8,128)(2,1)} %wq_hbm.1, bf16[2048,512]{1,0:T(8,128)(2,1)} %wk_hbm.1, bf16[2048,512]{1,0:T(8,128)(2,1)} %wv_hbm.1, bf16[512,2048]{1,0:T(8,128)(2,1)} %wo_hbm.1, f32[4]{0:T(128)} %lam_ref.1, f32[1,128]{1,0:T(1,128)} %bitcast.1), custom_call_target="tpu_custom_call" | custom-call | tf_op jit(solution)/shard_map/pallas_call | solution.py:523
  89.1 1.6 %copy.9 = bf16[48,2048]{1,0:T(8,128)(2,1)} copy(bf16[48,2048]{1,0:T(8,128)(2,1)} %shard_map.73) | data formatting | bytes 393216

commit v2 on v1

--- a/solution.py
+++ b/solution.py
@@ -14,6 +14,7 @@
 Y_OFFSET = (0, 1, 3, 2)
 BF16 = jnp.bfloat16
 F32 = jnp.float32
+LOG2E = 1.4426950408889634
 
 
 def kernel(
@@ -36,7 +37,6 @@
     kv,
     qw,
     top,
-    total,
     acc,
     nbuf,
     mixin,
@@ -151,18 +151,16 @@
     y_copy(2, 1).start()
     y_copy(1, 0).start()
 
-    def x_copies(s, o):
+    def x_copy(s, o, which):
         other = around(x, o, NX)
         source = around(x, -o, NX)
         to = device(z, other, c, y)
         mine = pl.ds(pl.multiple_of(s * group + x * rows, 16), rows)
         theirs = pl.ds(pl.multiple_of(s * group + source * rows, 16), rows)
-        return (
-            remote(send_kv.at[s, other], kv.at[0, mine], x_send.at[s, o], x_recv.at[s, o], to),
-            remote(send_q.at[s, other], qbuf.at[mine], q_send.at[s, o], q_recv.at[s, o], to),
-            remote(send_kv.at[s, other], kv.at[0, theirs], x_send.at[s, o], x_recv.at[s, o], to),
-            remote(send_q.at[s, other], qbuf.at[theirs], q_send.at[s, o], q_recv.at[s, o], to),
-        )
+        span = mine if which < 2 else theirs
+        if which % 2 == 0:
+            return remote(send_kv.at[s, other], kv.at[0, span], x_send.at[s, o], x_recv.at[s, o], to)
+        return remote(send_q.at[s, other], qbuf.at[span], q_send.at[s, o], q_recv.at[s, o], to)
 
     def project(s):
         first = tok[s, 0]
@@ -181,13 +179,13 @@
             send_kv[s, head, :, :128] = keys[:, cols]
             send_kv[s, head, :, 128:] = values[:, cols]
         for o in (2, 1, 3):
-            x_copies(s, o)[0].start()
+            x_copy(s, o, 0).start()
         kv[0, mine, :] = send_kv[s, x]
         found = product(2)
         for head in range(NX):
             send_q[s, head] = found[:, head * 128 : head * 128 + 128]
         for o in (2, 1, 3):
-            x_copies(s, o)[1].start()
+            x_copy(s, o, 1).start()
         qbuf[mine, :] = send_q[s, x]
 
     def ring_first(s, way):
@@ -211,7 +209,7 @@
 
     def launch(s):
         for o in (1, 3, 2):
-            x_copies(s, o)[2].wait_recv()
+            x_copy(s, o, 2).wait_recv()
         for way in range(2):
             copy = ring_first(s, way)
             if copy is not None:
@@ -309,21 +307,27 @@
 
     for s in range(NY):
         for o in (1, 3, 2):
-            x_copies(s, o)[3].wait_recv()
+            x_copy(s, o, 3).wait_recv()
     upper = lax.broadcasted_iota(jnp.int32, (128, 128), 0) < 64
 
     def build(t, carry):
-        block = qbuf[pl.ds(pl.multiple_of(t * 128, 128), 128), :].astype(F32) * (64**-0.5)
-        block = block.T
+        block = qbuf[pl.ds(pl.multiple_of(t * 128, 128), 128), :].astype(F32)
+        block = block.T * (64**-0.5 * LOG2E)
         nothing = jnp.zeros_like(block)
-        qw[t, :, :128] = jnp.where(upper, block, nothing).astype(BF16)
-        qw[t, :, 128:] = jnp.where(upper, nothing, block).astype(BF16)
+        for map_, part in enumerate((jnp.where(upper, block, nothing), jnp.where(upper, nothing, block))):
+            high = part.astype(BF16)
+            low = (part - high.astype(F32)).astype(BF16)
+            qw[t, :128, map_ * 128 : map_ * 128 + 128] = high
+            qw[t, 128:, map_ * 128 : map_ * 128 + 128] = low
         return carry
 
     lax.fori_loop(0, tiles, build, 0)
     top[...] = jnp.full_like(top, -1e30)
-    total[...] = jnp.zeros_like(total)
     acc[...] = jnp.zeros_like(acc)
+
+    ones = jnp.where(
+        lax.broadcasted_iota(jnp.int32, (16, 4 * group), 0) == 0, 1.0, 0.0
+    ).astype(BF16)
 
     def arrival(e, way):
         return remote(
@@ -383,16 +387,26 @@
             to_sibling(u - 2).wait_recv()
 
         keys = kv[u, :, :128]
-        values = kv[u, :, 128:].T
+        keys = jnp.concatenate([keys, keys], axis=1)
+        values = jnp.concatenate([kv[u, :, 128:].T, ones], axis=0)
+        scores = [jnp.dot(keys, qw[t], preferred_element_type=F32) for t in range(2)]
+        waiting = []
+
+        def add():
+            t, factor, weights = waiting.pop(0)
+            acc[t] = acc[t] * factor + jnp.dot(values, weights, preferred_element_type=F32)
+
         for t in range(tiles):
-            scores = jnp.dot(keys, qw[t], preferred_element_type=F32)
+            if t + 2 < tiles:
+                scores.append(jnp.dot(keys, qw[t + 2], preferred_element_type=F32))
+            block = scores.pop(0)
             before = top[t]
-            now = jnp.maximum(before, jnp.max(scores, axis=0, keepdims=True))
-            factor = jnp.exp(before - now)
-            expw = jnp.exp(scores - now)
+            now = jnp.maximum(before, jnp.max(block, axis=0, keepdims=True))
             top[t] = now
-            total[t] = total[t] * factor + jnp.sum(expw, axis=0, keepdims=True)
-            acc[t] = acc[t] * factor + jnp.dot(values, expw.astype(BF16), preferred_element_type=F32)
+            waiting.append((t, jnp.exp2(before - now), jnp.exp2(block - now).astype(BF16)))
+            if t > 0:
+                add()
+        add()
         return carry
 
     relay_at = events // 2
@@ -423,7 +437,7 @@
     gain = gain_ref[...]
 
     def finish(t, carry):
-        ratio = acc[t] / total[t]
+        ratio = acc[t, :128] / acc[t, 128:129]
         heads_out = ratio[:, :128] - mix * ratio[:, 128:]
         meansq = jnp.mean(heads_out * heads_out, axis=0, keepdims=True)
         normed = (heads_out * lax.rsqrt(meansq + 1e-06)).T * gain
@@ -474,9 +488,8 @@
         y_relay(part).wait_send()
     for s in range(NY):
         for o in (1, 2, 3):
-            copies = x_copies(s, o)
-            copies[0].wait_send()
-            copies[1].wait_send()
+            x_copy(s, o, 0).wait_send()
+            x_copy(s, o, 1).wait_send()
         for way in range(2):
             copy = ring_first(s, way)
             if copy is not None:
@@ -534,10 +547,9 @@
                 pltpu.VMEM((NY, NX, rows, 128), BF16),
                 pltpu.VMEM((queries, 128), BF16),
                 pltpu.VMEM((events + 2, 4 * group, 256), BF16),
-                pltpu.VMEM((tiles, 128, 256), BF16),
+                pltpu.VMEM((tiles, 256, 256), BF16),
                 pltpu.VMEM((tiles, 1, 256), F32),
-                pltpu.VMEM((tiles, 1, 256), F32),
-                pltpu.VMEM((tiles, 128, 256), F32),
+                pltpu.VMEM((tiles, 144, 256), F32),
                 pltpu.VMEM((queries, 128), BF16),
                 pltpu.VMEM((NX * NY, rows, 128), BF16),
                 dma((7,)),

time: 91.7 us -> 65.9 us (0.72)
  Pallas kernels: 89.1 us -> 64.1 us
    pallas_call x1, Pallas kernels: 89.1 us -> 64.1 us  [shards(): pl.pallas_call(functools.partial(kernel, nz, rows), out_shape=jax.ShapeDt...]
where the time goes in v2:
time: 65.9 us; the launch traced here: 65.8 us
  Pallas kernels  64.1 us (97%)
  local copies, waits for them, and re-layouts  1.62 us (2%)
    pallas_call x1, Pallas kernels, shards(): pl.pallas_call(functools.partial(kernel, nz, rows), out_shape=jax.ShapeDt...  64.1 us
    unnamed x1, local copies, waits for them, and re-layouts  1.62 us

profile of v2, /device:TPU:1, one launch (start us, length us, event | category | flops | bytes accessed | tf_op | source)
XLA Modules:
  0.0 65.8 jit_solution(14012882619604145901)
XLA Ops:
  0.0 64.1 %shard_map.73 = bf16[48,2048]{1,0:T(8,128)(2,1)} custom-call(bf16[48,2048]{1,0:T(8,128)(2,1)} %tok_hbm.1, bf16[2048,512]{1,0:T(8,128)(2,1)} %wq_hbm.1, bf16[2048,512]{1,0:T(8,128)(2,1)} %wk_hbm.1, bf16[2048,512]{1,0:T(8,128)(2,1)} %wv_hbm.1, bf16[512,2048]{1,0:T(8,128)(2,1)} %wo_hbm.1, f32[4]{0:T(128)} %lam_ref.1, f32[1,128]{1,0:T(1,128)} %bitcast.1), custom_call_target="tpu_custom_call" | custom-call | tf_op jit(solution)/shard_map/pallas_call | solution.py:536
  64.2 1.6 %copy.9 = bf16[48,2048]{1,0:T(8,128)(2,1)} copy(bf16[48,2048]{1,0:T(8,128)(2,1)} %shard_map.73) | data formatting | bytes 393216

commit v3 on v0

v3 whole, which is shorter than its diff:
```python
import functools

import jax
import jax.numpy as jnp
from jax import lax
from jax.experimental import pallas as pl
from jax.experimental.pallas import tpu as pltpu
from jax.sharding import PartitionSpec as P

MESH = pl.DeviceIdType.MESH
NX = 4
NY = 4
NC = 2
Y_OFFSET = (0, 1, 3, 2)
BF16 = jnp.bfloat16
F32 = jnp.float32
LOG2E = 1.4426950408889634
RIGHT = ((0, 1), (0, 2), (1, 1), (2, 1), (0, 3), (3, 1), (1, 2), (2, 2), (3, 2), (1, 3), (2, 3), (3, 3), (0, 4), (1, 4))
LEFT = RIGHT[:12] + ((2, 4), (3, 4))
EVENTS = len(RIGHT)


def kernel(
    nz,
    rows,
    sem_shapes,
    tok_hbm,
    wq_hbm,
    wk_hbm,
    wv_hbm,
    wo_hbm,
    lam_ref,
    gain_ref,
    out_ref,
    tok,
    wkvq,
    wo,
    send_kv,
    send_q,
    qbuf,
    kv,
    qw,
    top,
    acc,
    nbuf,
    mixin,
):
    def body(
        load_sem,
        y_send,
        y_recv,
        x_send,
        x_recv,
        q_send,
        q_recv,
        r_send,
        r_recv,
        s_send,
        s_recv,
        wo_send,
        wo_recv,
        wx_send,
        wx_recv,
        ws_send,
        ws_recv,
        o_send,
        o_recv,
    ):
        events = EVENTS
        depth = tok.shape[-1]
        group = NX * rows
        queries = NY * group
        tiles = queries // 128
        out_rows = wo_hbm.shape[0]
        out_cols = wo.shape[-1]

        sp = lax.axis_index("sp")
        y = lax.axis_index("tp")
        c = lax.rem(sp, NC)
        x = lax.rem(sp // NC, NX)
        z = sp // (NC * NX)

        def device(zz, xx, cc, yy):
            return {"sp": (zz * NX + xx) * NC + cc, "tp": yy}

        def around(value, step, count):
            return lax.rem(value + (step % count), count)

        def remote(src, dst, send, recv, where):
            return pltpu.make_async_remote_copy(
                src_ref=src,
                dst_ref=dst,
                send_sem=send,
                recv_sem=recv,
                device_id=where,
                device_id_type=MESH,
            )

        up = device(z, x, c, around(y, 1, NY))
        down = device(z, x, c, around(y, -1, NY))
        right = device(around(z, 1, nz), x, c, y)
        left = device(around(z, -1, nz), x, c, y)
        sibling = device(z, x, 1 - c, y)

        loads = []
        for part in range(2):
            loads.append(
                pltpu.make_async_copy(
                    tok_hbm.at[:, pl.ds(part * depth, depth)], tok.at[0, part], load_sem.at[part]
                )
            )
        weight_loads = [
            pltpu.make_async_copy(w, wkvq.at[i], load_sem.at[2 + i])
            for i, w in enumerate((wk_hbm, wv_hbm, wq_hbm))
        ]
        wo_loads = [
            pltpu.make_async_copy(
                wo_hbm.at[:, pl.ds(part * out_cols, out_cols)], wo.at[y, part], load_sem.at[5 + part]
            )
            for part in range(2)
        ]
        for copy in loads:
            copy.start()

        barrier = pltpu.get_barrier_semaphore()
        peers = [up, down, right, left, sibling, device(z, x, c, around(y, 2, NY))]
        peers += [device(z, around(x, ox, NX), c, y) for ox in range(1, NX)]
        for peer in peers:
            pl.semaphore_signal(barrier, inc=1, device_id=peer, device_id_type=MESH)
        for copy in weight_loads + wo_loads:
            copy.start()
        for copy in loads:
            copy.wait()
        pl.semaphore_wait(barrier, len(peers))

        def y_copy(slot):
            step = -Y_OFFSET[slot]
            where = device(z, x, c, around(y, step, NY))
            return remote(tok.at[0], tok.at[slot], y_send.at[slot], y_recv.at[slot], where)

        y_copy(1).start()
        y_copy(2).start()

        def x_copy(s, o, which):
            other = around(x, o, NX)
            source = around(x, -o, NX)
            to = device(z, other, c, y)
            mine = pl.ds(pl.multiple_of(s * group + x * rows, 16), rows)
            theirs = pl.ds(pl.multiple_of(s * group + source * rows, 16), rows)
            span = mine if which < 2 else theirs
            if which % 2 == 0:
                return remote(send_kv.at[s, other], kv.at[0, span], x_send.at[s, o], x_recv.at[s, o], to)
            return remote(send_q.at[s, other], qbuf.at[span], q_send.at[s, o], q_recv.at[s, o], to)

        def project(subs):
            def tokens(part):
                blocks = [tok[s, part] for s in subs]
                return blocks[0] if len(blocks) == 1 else jnp.concatenate(blocks, axis=0)

            first = tokens(0)
            second = tokens(1)

            def product(i):
                out = jnp.dot(first, wkvq[i, :depth, :], preferred_element_type=F32)
                out += jnp.dot(second, wkvq[i, depth:, :], preferred_element_type=F32)
                return out.astype(BF16)

            def mine(s):
                return pl.ds(pl.multiple_of(s * group + x * rows, 16), rows)

            keys = product(0)
            values = product(1)
            for at, s in enumerate(subs):
                span = slice(at * rows, at * rows + rows)
                for head in range(NX):
                    cols = slice(head * 128, head * 128 + 128)
                    send_kv[s, head, :, :128] = keys[span, cols]
                    send_kv[s, head, :, 128:] = values[span, cols]
                for o in (2, 1, 3):
                    x_copy(s, o, 0).start()
                kv[0, mine(s), :] = send_kv[s, x]
            found = product(2)
            for at, s in enumerate(subs):
                for head in range(NX):
                    send_q[s, head] = found[at * rows : at * rows + rows, head * 128 : head * 128 + 128]
                for o in (2, 1, 3):
                    x_copy(s, o, 1).start()
                qbuf[mine(s), :] = send_q[s, x]

        def place(e, way):
            return kv.at[2 + e // 2, pl.ds((e % 2 * 2 + way) * group, group)]

        def ring_first(s, way):
            event = (RIGHT, LEFT)[way].index((s, 1))
            return remote(
                kv.at[0, pl.ds(s * group, group)],
                place(event, way),
                r_send.at[events + s, way],
                r_recv.at[event, way],
                right if way == 0 else left,
            )

        def sibling_first(s):
            span = pl.ds(s * group, group)
            return remote(kv.at[0, span], kv.at[1, span], s_send.at[events + s], s_recv.at[events + s], sibling)

        def launch(s):
            for o in (1, 3, 2):
                x_copy(s, o, 2).wait_recv()
            for way in range(2):
                ring_first(s, way).start()
            sibling_first(s).start()

        size = out_rows // 4
        parity = lax.rem(x, 2)
        east = device(z, around(x, 1, NX), c, y)
        west = device(z, around(x, -1, NX), c, y)
        planes = [around(y, step, NY) for step in (-1, 1, 2)]

        def wo_rows(half_, chunk):
            return pl.ds(pl.multiple_of((half_ * 2 + chunk) * size, 16), size)

        def wo_copy(way, chunk):
            span = wo.at[y, c, wo_rows(parity, chunk)]
            return remote(
                span, span, wo_send.at[way, chunk], wo_recv.at[way, chunk], up if way == 0 else down
            )

        def wo_relay(chunk):
            span = wo.at[planes[chunk], c, wo_rows(parity, chunk)]
            return remote(
                span, span, wo_send.at[2, chunk], wo_recv.at[2, chunk], up if chunk == 0 else down
            )

        def wo_arrival(way, chunk):
            span = wo.at[planes[way], c, wo_rows(parity, chunk)]
            return remote(span, span, wo_send.at[way, chunk], wo_recv.at[way, chunk], up)

        def wo_across(way, chunk):
            span = wo.at[planes[way], c, wo_rows(parity, chunk)]
            return remote(
                span, span, wx_send.at[way, chunk], wx_recv.at[way, chunk], east if chunk == 0 else west
            )

        def wo_across_arrival(way, chunk):
            span = wo.at[planes[way], c, wo_rows(1 - parity, chunk)]
            return remote(span, span, wx_send.at[way, chunk], wx_recv.at[way, chunk], east)

        def wo_sibling(way, core):
            span = wo.at[planes[way], core]
            return remote(span, span, ws_send.at[way], ws_recv.at[way], sibling)

        def wo_pass(way, chunk):
            wo_arrival(way, chunk).wait_recv()
            wo_across(way, chunk).start()

        def arrival(e, way):
            return remote(
                kv.at[0, pl.ds(0, group)], place(e, way), r_send.at[e, way], r_recv.at[e, way], right
            )

        def forward(e, way):
            order = (RIGHT, LEFT)[way]
            piece, distance = order[e]
            if (piece, distance + 1) not in order:
                return None
            target = order.index((piece, distance + 1))
            return remote(
                place(e, way),
                place(target, way),
                r_send.at[e, way],
                r_recv.at[target, way],
                right if way == 0 else left,
            )

        def to_sibling(e):
            span = pl.ds(e % 2 * 2 * group, 2 * group)
            return remote(
                kv.at[2 + e // 2, span], kv.at[9 + e // 2, span], s_send.at[e], s_recv.at[e], sibling
            )

        def receive(e):
            for way in range(2):
                arrival(e, way).wait_recv()
                copy = forward(e, way)
                if copy is not None:
                    copy.start()
            to_sibling(e).start()

        upper = lax.broadcasted_iota(jnp.int32, (128, 128), 0) < 64

        def build(t, carry):
            block = qbuf[pl.ds(pl.multiple_of(t * 128, 128), 128), :].astype(F32)
            block = block.T * (64**-0.5 * LOG2E)
            nothing = jnp.zeros_like(block)
            for map_, part in enumerate((jnp.where(upper, block, nothing), jnp.where(upper, nothing, block))):
                high = part.astype(BF16)
                low = (part - high.astype(F32)).astype(BF16)
                qw[t, :128, map_ * 128 : map_ * 128 + 128] = high
                qw[t, 128:, map_ * 128 : map_ * 128 + 128] = low
            return carry

        def queries_of(subs):
            for s in subs:
                for o in (1, 3, 2):
                    x_copy(s, o, 3).wait_recv()

        for copy in weight_loads:
            copy.wait()
        project([0])
        launch(0)
        y_copy(3).start()
        y_copy(1).wait_recv()
        y_copy(2).wait_recv()
        project([1, 2])
        for copy in wo_loads:
            copy.wait()
        for way, chunk in ((0, 0), (1, 1), (0, 1), (1, 0)):
            wo_copy(way, chunk).start()
        receive(0)
        launch(1)
        launch(2)
        y_copy(3).wait_recv()
        project([3])
        receive(1)
        queries_of((0, 1, 2))
        early = 3 * group // 128
        lax.fori_loop(0, early, build, 0)
        ones = jnp.where(
            lax.broadcasted_iota(jnp.int32, (16, 4 * group), 0) == 0, 1.0, 0.0
        ).astype(BF16)
        top[...] = jnp.full_like(top, -1e30)
        acc[...] = jnp.zeros_like(acc)
        launch(3)
        queries_of((3,))
        lax.fori_loop(early, tiles, build, 0)

        def attend(units):
            for u in units:

                @pl.when(u == 1)
                def _():
                    for s in range(NY):
                        sibling_first(s).wait_recv()

                @pl.when(u >= 9)
                def _():
                    for at in range(2):
                        e = 2 * (u - 9) + at
                        span = pl.ds(at * 2 * group, 2 * group)
                        remote(
                            kv.at[0, span], kv.at[u, span], s_send.at[e], s_recv.at[e], sibling
                        ).wait_recv()

            keys = []
            values = []
            for u in units:
                block = kv[u, :, :128]
                keys.append(jnp.concatenate([block, block], axis=1))
                values.append(jnp.concatenate([kv[u, :, 128:].T, ones], axis=0))
            items = [(i, t) for i in range(len(units)) for t in range(tiles)]

            def score(item):
                i, t = item
                return jnp.dot(keys[i], qw[t], preferred_element_type=F32)

            scores = [score(item) for item in items[:2]]
            waiting = []

            def add():
                i, t, factor, weights = waiting.pop(0)
                acc[t] = acc[t] * factor + jnp.dot(values[i], weights, preferred_element_type=F32)

            for at, (i, t) in enumerate(items):
                if at + 2 < len(items):
                    scores.append(score(items[at + 2]))
                block = scores.pop(0)
                before = top[t]
                now = jnp.maximum(before, jnp.max(block, axis=0, keepdims=True))
                top[t] = now
                waiting.append((i, t, jnp.exp2(before - now), jnp.exp2(block - now).astype(BF16)))
                if at > 0:
                    add()
            add()

        def pick(at, numbers):
            found = jnp.int32(numbers[-1])
            for i in range(len(numbers) - 2, -1, -1):
                found = jnp.where(at == i, numbers[i], found)
            return found

        def step(k, carry):
            @pl.when(k == 1)
            def _():
                receive(2)
                receive(3)
                for way in range(2):
                    wo_arrival(way, way).wait_recv()
                    wo_relay(way).start()
                    wo_across(way, way).start()

            @pl.when(k == 2)
            def _():
                receive(4)
                receive(5)

            @pl.when(k == 3)
            def _():
                receive(6)
                for way in range(2):
                    wo_pass(way, 1 - way)

            attend([pick(k, (0, 3, 1, 10)), pick(k, (2, 9, 4, 11))])
            return carry

        lax.fori_loop(0, 4, step, 0)

        def last(i, carry):
            for at in range(5):

                @pl.when(i == at)
                def _(at=at):
                    receive(7 + at)

            @pl.when(i == 0)
            def _():
                for chunk in range(2):
                    wo_pass(2, chunk)

            @pl.when(i == 6)
            def _():
                receive(12)
                receive(13)

            @pl.when(i == 4)
            def _():
                for way in range(3):
                    for chunk in range(2):
                        wo_across_arrival(way, chunk).wait_recv()
                    wo_sibling(way, c).start()

            attend([pick(i, (5, 12, 6, 13, 7, 14, 8, 15))])
            return carry

        lax.fori_loop(0, 8, last, 0)

        mix = lam_ref[x]
        gain = gain_ref[...]

        def finish(t, carry):
            ratio = acc[t, :128] / acc[t, 128:129]
            heads_out = ratio[:, :128] - mix * ratio[:, 128:]
            meansq = jnp.mean(heads_out * heads_out, axis=0, keepdims=True)
            normed = (heads_out * lax.rsqrt(meansq + 1e-06)).T * gain
            nbuf[pl.ds(pl.multiple_of(t * 128, 128), 128), :] = normed.astype(BF16)
            return carry

        lax.fori_loop(0, tiles, finish, 0, unroll=True)

        def o_copy(s, o, arriving):
            other = around(x, o, NX)
            span = pl.ds(pl.multiple_of(s * group + other * rows, 16), rows)
            if arriving:
                slot = around(y, -Y_OFFSET[s], NY) * NX + around(x, -o, NX)
            else:
                slot = y * NX + x
            return remote(
                nbuf.at[span],
                mixin.at[slot],
                o_send.at[s, o],
                o_recv.at[s, o],
                device(z, other, c, around(y, Y_OFFSET[s], NY)),
            )

        exchanges = [(s, o) for s in (3, 1, 2, 0) for o in (2, 1, 3, 0) if (s, o) != (0, 0)]
        for s, o in exchanges:
            o_copy(s, o, False).start()
        mixin[y * NX + x] = nbuf[pl.ds(pl.multiple_of(x * rows, 16), rows), :]

        for way in range(3):
            wo_sibling(way, 1 - c).wait_recv()
        mixed = [jnp.zeros((rows, out_cols), F32) for _ in range(2)]
        for s in (0, 1, 2, 3):
            for o in (0, 1, 3, 2):
                if (s, o) != (0, 0):
                    o_copy(s, o, True).wait_recv()
            origin = around(y, -Y_OFFSET[s], NY)
            normed = jnp.concatenate([mixin[origin * NX + i] for i in range(NX)], axis=1)
            for part in range(2):
                mixed[part] += jnp.dot(normed, wo[origin, part], preferred_element_type=F32)
        for part in range(2):
            out_ref[:, part * out_cols : (part + 1) * out_cols] = mixed[part].astype(BF16)

        for slot in (1, 2, 3):
            y_copy(slot).wait_send()
        for s in range(NY):
            for o in (1, 2, 3):
                x_copy(s, o, 0).wait_send()
                x_copy(s, o, 1).wait_send()
            for way in range(2):
                ring_first(s, way).wait_send()
            sibling_first(s).wait_send()

        for e in range(events):
            for way in range(2):
                copy = forward(e, way)
                if copy is not None:
                    copy.wait_send()
            to_sibling(e).wait_send()
        for way in range(3):
            for chunk in range(2):
                if way < 2:
                    wo_copy(way, chunk).wait_send()
                wo_across(way, chunk).wait_send()
            wo_sibling(way, c).wait_send()
        for chunk in range(2):
            wo_relay(chunk).wait_send()
        for s, o in exchanges:
            o_copy(s, o, False).wait_send()

    pl.run_scoped(body, *sem_shapes)


def solution(mesh):
    nz = mesh.shape["sp"] // (NX * NC)
    assert nz == 8

    def shards(tokens, w_query, w_key, w_value, w_out, mix_weight, out_gain):
        rows, width = tokens.shape
        cols = w_query.shape[1]
        group = NX * rows
        queries = NY * group
        tiles = queries // 128
        events = EVENTS
        dma = pltpu.SemaphoreType.DMA
        anywhere = pl.BlockSpec(memory_space=pl.ANY)
        semaphores = [
            dma((7,)),
            dma((4,)),
            dma((4,)),
            dma((4, 4)),
            dma((4, 4)),
            dma((4, 4)),
            dma((4, 4)),
            dma((events + 4, 2)),
            dma((events, 2)),
            dma((events + 4,)),
            dma((events + 4,)),
            dma((3, 2)),
            dma((3, 2)),
            dma((3, 2)),
            dma((3, 2)),
            dma((3,)),
            dma((3,)),
            dma((4, 4)),
            dma((4, 4)),
        ]
        return pl.pallas_call(
            functools.partial(kernel, nz, rows, semaphores),
            out_shape=jax.ShapeDtypeStruct((rows, width), BF16),
            in_specs=[anywhere] * 5
            + [pl.BlockSpec(memory_space=pltpu.SMEM), pl.BlockSpec(memory_space=pltpu.VMEM)],
            out_specs=pl.BlockSpec(memory_space=pltpu.VMEM),
            scratch_shapes=[
                pltpu.VMEM((NY, 2, rows, width // 2), BF16),
                pltpu.VMEM((3, width, cols), BF16),
                pltpu.VMEM((NY, 2, w_out.shape[0], width // 2), BF16),
                pltpu.VMEM((NY, NX, rows, 256), BF16),
                pltpu.VMEM((NY, NX, rows, 128), BF16),
                pltpu.VMEM((queries, 128), BF16),
                pltpu.VMEM((events + 2, 4 * group, 256), BF16),
                pltpu.VMEM((tiles, 256, 256), BF16),
                pltpu.VMEM((tiles, 1, 256), F32),
                pltpu.VMEM((tiles, 144, 256), F32),
                pltpu.VMEM((queries, 128), BF16),
                pltpu.VMEM((NX * NY, rows, 128), BF16),
            ],
            compiler_params=pltpu.CompilerParams(
                collective_id=0,
                has_side_effects=True,
                vmem_limit_bytes=56 * 1024 * 1024,
            ),
        )(tokens, w_query, w_key, w_value, w_out, mix_weight, out_gain.reshape(1, -1))

    in_specs = (
        P(("sp", "tp"), None),
        P(None, "tp"),
        P(None, "tp"),
        P(None, "tp"),
        P("tp", None),
        P("tp"),
        P(),
    )
    return jax.shard_map(
        shards, mesh=mesh, in_specs=in_specs, out_specs=P(("sp", "tp"), None), check_vma=False
    )
```

time: 398 us -> 64.8 us (0.16)
  local copies, waits for them, and re-layouts: 136 us -> 1.62 us
  waiting for transfers between devices: 86.8 us -> 0 us
  matrix products: 81.7 us -> 0 us
  Pallas kernels: 0 us -> 63.1 us
  other arithmetic: 44.3 us -> 0 us
  blocking collectives: 31.9 us -> 0 us
  between operations: 13.5 us -> 0.01 us
    all_gather x2 -> x0, waiting for transfers between devices: 86.8 us -> none  [the longest x1 86.8 us: shards(): lax.all_gather(keys, 'sp', axis=0, tiled=True)]
    dot_general x16 -> x0, matrix products: 81.7 us -> none  [the longest x6 47.4 us: step(): jnp.einsum('qhmd,khmd->hmqk', query_four, key_blk, preferred_element_type...]
    pallas_call x0 -> x1, Pallas kernels: none -> 63.1 us  [shards(): pl.pallas_call(functools.partial(kernel, nz, rows, semaphores), out_shape...]
    reshape x2 -> x0, local copies, waits for them, and re-layouts: 62.8 us -> none  [the longest x1 44.6 us: shards(): key_blocks = all_keys.reshape(rows // group, group, heads_here, 2, head_dim)]
    unnamed x8 -> x1, local copies, waits for them, and re-layouts: 58.7 us -> 1.62 us
    reduce_sum x8 -> x0, other arithmetic: 44 us -> none  [the longest x6 41.6 us: step(): running_sum = running_sum * factor + jnp.sum(expw, axis=-1)]
    all_to_all x2 -> x0, blocking collectives: 31.9 us -> none  [the longest x1 16.2 us: from_everyone(): return lax.all_to_all(copies, axis, split_axis=0, concat_axis=0, tiled=True)]
    dynamic_slice x6 -> x0, local copies, waits for them, and re-layouts: 12.9 us -> none  [shards(): carry, unused = lax.scan(step, carry, (key_blocks, value_blocks))]
  transfers between devices with their start and end apart: 2 -> 0, of which waited for: 1 -> 0; matrix products, arithmetic and copies ran while one was open for 28% -> 0% of each run, Pallas kernels for 0% -> 0%
where the time goes in v3:
time: 64.8 us; the launch traced here: 64.7 us
  Pallas kernels  63.1 us (97%)
  local copies, waits for them, and re-layouts  1.62 us (2%)
    pallas_call x1, Pallas kernels, shards(): pl.pallas_call(functools.partial(kernel, nz, rows, semaphores), out_shape...  63.1 us
    unnamed x1, local copies, waits for them, and re-layouts  1.62 us

profile of v3, /device:TPU:1, one launch (start us, length us, event | category | flops | bytes accessed | tf_op | source)
XLA Modules:
  0.0 64.7 jit_solution(14462597954033132168)
XLA Ops:
  0.0 63.1 %shard_map.73 = bf16[48,2048]{1,0:T(8,128)(2,1)} custom-call(bf16[48,2048]{1,0:T(8,128)(2,1)} %tok_hbm.1, bf16[2048,512]{1,0:T(8,128)(2,1)} %wq_hbm.1, bf16[2048,512]{1,0:T(8,128)(2,1)} %wk_hbm.1, bf16[2048,512]{1,0:T(8,128)(2,1)} %wv_hbm.1, bf16[512,2048]{1,0:T(8,128)(2,1)} %wo_hbm.1, f32[4]{0:T(128)} %lam_ref.1, f32[1,128]{1,0:T(1,128)} %bitcast.1), custom_call_target="tpu_custom_call" | custom-call | tf_op jit(solution)/shard_map/pallas_call | solution.py:558
  63.1 1.6 %copy.9 = bf16[48,2048]{1,0:T(8,128)(2,1)} copy(bf16[48,2048]{1,0:T(8,128)(2,1)} %shard_map.73) | data formatting | bytes 393216

commit v4 on v3

--- a/solution.py
+++ b/solution.py
@@ -407,20 +407,21 @@
             @pl.when(k == 3)
             def _():
                 receive(6)
+                receive(7)
                 for way in range(2):
                     wo_pass(way, 1 - way)
 
-            attend([pick(k, (0, 3, 1, 10)), pick(k, (2, 9, 4, 11))])
+            attend([pick(k, (0, 3, 1, 10)), pick(k, (2, 9, 4, 5))])
             return carry
 
         lax.fori_loop(0, 4, step, 0)
 
         def last(i, carry):
-            for at in range(5):
+            for at in range(4):
 
                 @pl.when(i == at)
                 def _(at=at):
-                    receive(7 + at)
+                    receive(8 + at)
 
             @pl.when(i == 0)
             def _():
@@ -439,7 +440,7 @@
                         wo_across_arrival(way, chunk).wait_recv()
                     wo_sibling(way, c).start()
 
-            attend([pick(i, (5, 12, 6, 13, 7, 14, 8, 15))])
+            attend([pick(i, (11, 6, 12, 7, 13, 14, 8, 15))])
             return carry
 
         lax.fori_loop(0, 8, last, 0)

time: 64.8 us -> 66.6 us (1.028)
  Pallas kernels: 63.1 us -> 64.9 us
    pallas_call x1, Pallas kernels: 63.1 us -> 64.9 us  [shards(): pl.pallas_call(functools.partial(kernel, nz, rows, semaphores), out_shape...]
where the time goes in v4:
time: 66.6 us; the launch traced here: 66.5 us
  Pallas kernels  64.9 us (97%)
  local copies, waits for them, and re-layouts  1.62 us (2%)
    pallas_call x1, Pallas kernels, shards(): pl.pallas_call(functools.partial(kernel, nz, rows, semaphores), out_shape...  64.9 us
    unnamed x1, local copies, waits for them, and re-layouts  1.62 us

profile of v4, /device:TPU:1, one launch (start us, length us, event | category | flops | bytes accessed | tf_op | source)
XLA Modules:
  0.0 66.5 jit_solution(6072490822052617710)
XLA Ops:
  0.0 64.9 %shard_map.73 = bf16[48,2048]{1,0:T(8,128)(2,1)} custom-call(bf16[48,2048]{1,0:T(8,128)(2,1)} %tok_hbm.1, bf16[2048,512]{1,0:T(8,128)(2,1)} %wq_hbm.1, bf16[2048,512]{1,0:T(8,128)(2,1)} %wk_hbm.1, bf16[2048,512]{1,0:T(8,128)(2,1)} %wv_hbm.1, bf16[512,2048]{1,0:T(8,128)(2,1)} %wo_hbm.1, f32[4]{0:T(128)} %lam_ref.1, f32[1,128]{1,0:T(1,128)} %bitcast.1), custom_call_target="tpu_custom_call" | custom-call | tf_op jit(solution)/shard_map/pallas_call | solution.py:559
  64.9 1.6 %copy.9 = bf16[48,2048]{1,0:T(8,128)(2,1)} copy(bf16[48,2048]{1,0:T(8,128)(2,1)} %shard_map.73) | data formatting | bytes 393216

commit v5 on v3

--- a/solution.py
+++ b/solution.py
@@ -44,6 +44,7 @@
     acc,
     nbuf,
     mixin,
+    result,
 ):
     def body(
         load_sem,
@@ -133,13 +134,16 @@
             copy.wait()
         pl.semaphore_wait(barrier, len(peers))
 
-        def y_copy(slot):
+        def y_copy(slot, part):
             step = -Y_OFFSET[slot]
             where = device(z, x, c, around(y, step, NY))
-            return remote(tok.at[0], tok.at[slot], y_send.at[slot], y_recv.at[slot], where)
-
-        y_copy(1).start()
-        y_copy(2).start()
+            return remote(
+                tok.at[0, part], tok.at[slot, part], y_send.at[slot, part], y_recv.at[slot, part], where
+            )
+
+        for part in range(2):
+            y_copy(1, part).start()
+            y_copy(2, part).start()
 
         def x_copy(s, o, which):
             other = around(x, o, NX)
@@ -157,19 +161,26 @@
                 blocks = [tok[s, part] for s in subs]
                 return blocks[0] if len(blocks) == 1 else jnp.concatenate(blocks, axis=0)
 
+            def arrive(part):
+                for s in subs:
+                    if s:
+                        y_copy(s, part).wait_recv()
+
+            def product(i, part, block):
+                weights = wkvq[i, part * depth : (part + 1) * depth, :]
+                return jnp.dot(block, weights, preferred_element_type=F32)
+
+            arrive(0)
             first = tokens(0)
+            sums = [product(i, 0, first) for i in range(3)]
+            arrive(1)
             second = tokens(1)
-
-            def product(i):
-                out = jnp.dot(first, wkvq[i, :depth, :], preferred_element_type=F32)
-                out += jnp.dot(second, wkvq[i, depth:, :], preferred_element_type=F32)
-                return out.astype(BF16)
 
             def mine(s):
                 return pl.ds(pl.multiple_of(s * group + x * rows, 16), rows)
 
-            keys = product(0)
-            values = product(1)
+            keys = (sums[0] + product(0, 1, second)).astype(BF16)
+            values = (sums[1] + product(1, 1, second)).astype(BF16)
             for at, s in enumerate(subs):
                 span = slice(at * rows, at * rows + rows)
                 for head in range(NX):
@@ -179,7 +190,7 @@
                 for o in (2, 1, 3):
                     x_copy(s, o, 0).start()
                 kv[0, mine(s), :] = send_kv[s, x]
-            found = product(2)
+            found = (sums[2] + product(2, 1, second)).astype(BF16)
             for at, s in enumerate(subs):
                 for head in range(NX):
                     send_q[s, head] = found[at * rows : at * rows + rows, head * 128 : head * 128 + 128]
@@ -309,9 +320,8 @@
             copy.wait()
         project([0])
         launch(0)
-        y_copy(3).start()
-        y_copy(1).wait_recv()
-        y_copy(2).wait_recv()
+        for part in range(2):
+            y_copy(3, part).start()
         project([1, 2])
         for copy in wo_loads:
             copy.wait()
@@ -320,7 +330,6 @@
         receive(0)
         launch(1)
         launch(2)
-        y_copy(3).wait_recv()
         project([3])
         receive(1)
         queries_of((0, 1, 2))
@@ -488,11 +497,21 @@
             normed = jnp.concatenate([mixin[origin * NX + i] for i in range(NX)], axis=1)
             for part in range(2):
                 mixed[part] += jnp.dot(normed, wo[origin, part], preferred_element_type=F32)
+        stores = []
         for part in range(2):
-            out_ref[:, part * out_cols : (part + 1) * out_cols] = mixed[part].astype(BF16)
-
+            cols = slice(part * out_cols, (part + 1) * out_cols)
+            result[:, cols] = mixed[part].astype(BF16)
+            span = pl.ds(part * out_cols, out_cols)
+            stores.append(
+                pltpu.make_async_copy(result.at[:, span], out_ref.at[:, span], load_sem.at[part])
+            )
+            stores[-1].start()
+
+        for copy in stores:
+            copy.wait()
         for slot in (1, 2, 3):
-            y_copy(slot).wait_send()
+            for part in range(2):
+                y_copy(slot, part).wait_send()
         for s in range(NY):
             for o in (1, 2, 3):
                 x_copy(s, o, 0).wait_send()
@@ -536,8 +555,8 @@
         anywhere = pl.BlockSpec(memory_space=pl.ANY)
         semaphores = [
             dma((7,)),
-            dma((4,)),
-            dma((4,)),
+            dma((4, 2)),
+            dma((4, 2)),
             dma((4, 4)),
             dma((4, 4)),
             dma((4, 4)),
@@ -560,7 +579,7 @@
             out_shape=jax.ShapeDtypeStruct((rows, width), BF16),
             in_specs=[anywhere] * 5
             + [pl.BlockSpec(memory_space=pltpu.SMEM), pl.BlockSpec(memory_space=pltpu.VMEM)],
-            out_specs=pl.BlockSpec(memory_space=pltpu.VMEM),
+            out_specs=anywhere,
             scratch_shapes=[
                 pltpu.VMEM((NY, 2, rows, width // 2), BF16),
                 pltpu.VMEM((3, width, cols), BF16),
@@ -574,6 +593,7 @@
                 pltpu.VMEM((tiles, 144, 256), F32),
                 pltpu.VMEM((queries, 128), BF16),
                 pltpu.VMEM((NX * NY, rows, 128), BF16),
+                pltpu.VMEM((rows, width), BF16),
             ],
             compiler_params=pltpu.CompilerParams(
                 collective_id=0,

time: 64.8 us -> 64.8 us (level)
  no operation moved by 1% of the time
where the time goes in v5:
time: 64.8 us; the launch traced here: 64.7 us
  Pallas kernels  63 us (97%)
  local copies, waits for them, and re-layouts  1.62 us (2%)
    pallas_call x1, Pallas kernels, shards(): pl.pallas_call(functools.partial(kernel, nz, rows, semaphores), out_shape...  63 us
    unnamed x1, local copies, waits for them, and re-layouts  1.62 us

profile of v5, /device:TPU:1, one launch (start us, length us, event | category | flops | bytes accessed | tf_op | source)
XLA Modules:
  0.0 64.7 jit_solution(11888779064019838176)
XLA Ops:
  0.0 63.0 %shard_map.73 = bf16[48,2048]{1,0:T(8,128)(2,1)} custom-call(bf16[48,2048]{1,0:T(8,128)(2,1)} %tok_hbm.1, bf16[2048,512]{1,0:T(8,128)(2,1)} %wq_hbm.1, bf16[2048,512]{1,0:T(8,128)(2,1)} %wk_hbm.1, bf16[2048,512]{1,0:T(8,128)(2,1)} %wv_hbm.1, bf16[512,2048]{1,0:T(8,128)(2,1)} %wo_hbm.1, f32[4]{0:T(128)} %lam_ref.1, f32[1,128]{1,0:T(1,128)} %bitcast.1), custom_call_target="tpu_custom_call" | custom-call | tf_op jit(solution)/shard_map/pallas_call | solution.py:577
  63.0 1.6 %copy.9 = bf16[48,2048]{1,0:T(8,128)(2,1)} copy(bf16[48,2048]{1,0:T(8,128)(2,1)} %shard_map.73) | data formatting | bytes 393216
